TPU v7x, 32 devices: a whole 2x2x4 slice. The times are simulated.
32 devices in a mesh: ep: 8 (over z, x), tp: 4 (over y, core).
Axes of the slice: x: 2, y: 2, z: 4, core: 2. Of those that a mesh axis runs over, the one named last changes fastest.
Arguments:
- tokens: bfloat16 [1024, 4096], P('ep', 'tp'), may hold values from -16 to 16
- expert_ids: int32 [1024, 2], P('ep'), may hold values from 0 to 7, as said below
- group_weight: float32 [1024], P('ep'), may hold values from 0.25 to 1
- expert_weight: float32 [1024, 2], P('ep'), may hold values from 0.1 to 1
- w_gate: bfloat16 [8, 4096, 512], P('ep', None, 'tp'), may hold values from -0.09375 to 0.09375
- w_up: bfloat16 [8, 4096, 512], P('ep', None, 'tp'), may hold values from -0.09375 to 0.09375
- w_down: bfloat16 [8, 512, 4096], P('ep', None, 'tp'), may hold values from -0.5 to 0.5
- norm_gain: float32 [4096], P('tp'), may hold values from 0.1 to 1.9
- norm_bias: float32 [4096], P('tp'), may hold values from -3 to 3
Outputs:
- normed: bfloat16 [1024, 4096], P('ep', 'tp')
Inputs may be any that keep to these rules, and one draw needn't show every extreme that they name: `expert_ids`: each row names 2 different experts of one group, a group being 2 consecutive ids; in the rows of one ep index each group is named by a 4-th of the rows. In the rows of one ep index no expert is named more than 32 times, and in every group one expert is named exactly 32 times in the rows of every ep index.
All inputs are finite; a program needn't handle non-finite values.
Results may differ from a plain program's by a relative error of at most 0.0045.
Values may be sent and summed in bfloat16 or wider, within the bound.
A program may use at most 64 MiB of HBM per device.

v0:
```python
import jax
import jax.numpy as jnp
from jax import lax
from jax.sharding import PartitionSpec as P

D = 4096
GROUPS = 4
TOP_K = 2
residual_scale = 2.0**0.5
norm_eps = 1e-05


def on_device(
    tokens, expert_ids, group_weight, expert_weight, w_gate, w_up, w_down, norm_gain, norm_bias
):
    tok_count = tokens.shape[0]
    expert_count = lax.axis_size("ep")
    capacity = min(tok_count // GROUPS, 3 * TOP_K * tok_count // (2 * expert_count))
    pair_count = tok_count * TOP_K
    flat_ids = expert_ids.reshape(pair_count)
    one_hot = (flat_ids[:, None] == jnp.arange(expert_count, dtype=jnp.int32)[None, :]).astype(
        jnp.float32
    )
    earlier = (jnp.arange(pair_count)[:, None] > jnp.arange(pair_count)[None, :]).astype(
        jnp.float32
    )
    prior_counts = jnp.dot(
        earlier, one_hot, preferred_element_type=jnp.float32, precision=lax.Precision.HIGHEST
    )
    slot_index = jnp.sum(prior_counts * one_hot, axis=1).astype(jnp.int32)
    position = flat_ids * capacity + slot_index
    owner_token = jnp.arange(pair_count, dtype=jnp.int32) // TOP_K
    slot_table = (
        jnp.full((expert_count * capacity,), tok_count, jnp.int32).at[position].set(owner_token)
    )
    gate_local = w_gate[0]
    up_local = w_up[0]
    down_local = w_down[0]
    padded = jnp.concatenate([tokens, jnp.zeros((1, tokens.shape[1]), tokens.dtype)], axis=0)
    outgoing = padded[slot_table].reshape(expert_count, capacity, tokens.shape[1])
    arrived = lax.all_to_all(outgoing, "ep", split_axis=0, concat_axis=0, tiled=True)
    sources, slot_count, slice_width = arrived.shape
    row_block = arrived.reshape(sources * slot_count, slice_width)
    row_piece = lax.all_gather(row_block, "tp", axis=1, tiled=True)
    gate_sum = jnp.dot(row_piece, gate_local, preferred_element_type=jnp.float32)
    up_sum = jnp.dot(row_piece, up_local, preferred_element_type=jnp.float32)
    hidden = (jax.nn.silu(gate_sum) * up_sum).astype(jnp.bfloat16)
    result = jnp.dot(
        lax.all_gather(hidden, "tp", axis=1, tiled=True),
        down_local,
        preferred_element_type=jnp.float32,
    )
    result = result.astype(jnp.bfloat16).reshape(sources, slot_count, down_local.shape[1])
    returned = lax.all_to_all(result, "ep", split_axis=0, concat_axis=0, tiled=True)
    flat_rows = returned.reshape(expert_count * capacity, returned.shape[2])
    picked = flat_rows[position].reshape(tok_count, TOP_K, returned.shape[2]).astype(jnp.float32)
    share_weight = (
        group_weight[:, None] * expert_weight / jnp.sum(expert_weight, axis=1, keepdims=True)
    )
    routed = jnp.einsum("tk,tkd->td", share_weight, picked)
    mixed = residual_scale * tokens.astype(jnp.float32) + routed
    first_sum, second_sum = lax.psum((jnp.sum(mixed, axis=1), jnp.sum(mixed * mixed, axis=1)), "tp")
    center = first_sum / D
    spread = second_sum / D - center * center
    centered = mixed - center[:, None]
    normed = (
        centered * lax.rsqrt(spread + norm_eps)[:, None] * norm_gain[None, :] + norm_bias[None, :]
    )
    return normed.astype(jnp.bfloat16)


def solution(mesh):
    return jax.shard_map(
        on_device,
        mesh=mesh,
        in_specs=(
            P("ep", "tp"),
            P("ep", None),
            P("ep"),
            P("ep", None),
            P("ep", None, "tp"),
            P("ep", None, "tp"),
            P("ep", None, "tp"),
            P("tp"),
            P("tp"),
        ),
        out_specs=P("ep", "tp"),
        check_vma=False,
    )
```

profile of v0, /device:TPU:0, one launch (start us, length us, event | category | flops | bytes accessed | tf_op | source)
XLA Modules:
  0.0 102.6 jit_solution(2581811494604423040)
XLA Ops:
  6.5 0.9 copy.11
  7.4 0.7 broadcast_multiply_fusion
  8.1 0.1 eq.15
  8.2 0.2 fusion.1
  8.5 0.1 copy.10
  8.6 0.1 mul.68
  8.7 1.4 %scatter_custom_fusion = s32[256]{0:T(256)S(1)} fusion(s32[256]{0:T(256)S(1)} %bitcast.33, s32[256]{0:T(256)S(1)} %and_select_fusion, s32[]{:T(128)} %constant.31.clone.1), kind=kCustom, calls=%fused_computation.30 | custom fusion | bytes 1028 | tf_op jit(solution)/shard_map/scatter | solution.py:34
  10.1 1.0 concatenate.3
  11.1 1.2 %gather_fusion = bf16[256,1024]{1,0:T(8,128)(2,1)S(1)} fusion(bf16[129,1024]{1,0:T(8,128)(2,1)S(1)} %concatenate.3, s32[1024]{0:T(1024)S(1)} %pad_clamp_fusion.1), kind=kCustom, calls=%fused_computation | custom fusion | bytes 1049600 | tf_op jit(solution)/shard_map/gather | solution.py:40
  12.3 21.7 %all_to_all.10 = bf16[8,32,1024]{2,1,0:T(8,128)(2,1)} all-to-all(bf16[8,32,1024]{2,1,0:T(8,128)(2,1)S(1)} %bitcast.31), channel_id=1, replica_groups=mesh['ep'=8,'tp'=4] {'ep'}, dimensions={0} | all-to-all | bytes 1048576 | tf_op jit(solution)/shard_map/all_to_all | solution.py:41
  34.0 21.8 %all-gather.2.cloned.1.call-done = bf16[256,4096]{1,0:T(8,128)(2,1)} async-done(((bf16[256,1024]{1,0:T(8,128)(2,1)}), bf16[256,4096]{1,0:T(8,128)(2,1)}) %all-gather.2.cloned.1.call-update) | async-done | bytes 2097168 | tf_op jit(solution)/shard_map/all_gather | solution.py:44
  55.8 2.5 %fusion.4 = f32[256,128]{1,0:T(8,128)S(1)} fusion(bf16[256,4096]{1,0:T(8,128)(2,1)} %all-gather.2.cloned.1.call-done, bf16[1,4096,128]{2,1,0:T(8,128)(2,1)S(1)} %copy-done.3), kind=kOutput, calls=%fused_computation.10 | convolution fusion | flops 268435456 | bytes 3276800 | tf_op jit(solution)/shard_map/dot_general | solution.py:45
  58.3 0.7 fusion
  59.0 5.8 %all_gather.7 = bf16[256,512]{1,0:T(8,128)(2,1)S(1)} all-gather(bf16[256,128]{1,0:T(8,128)(2,1)S(1)} %fusion), channel_id=1, replica_groups=mesh['ep'=8,'tp'=4] {'tp'}, dimensions={1}, use_global_device_ids=true | all-gather | bytes 327680 | tf_op jit(solution)/shard_map/all_gather | solution.py:49
  64.8 1.3 %convolution_convert_fusion = bf16[256,1024]{1,0:T(8,128)(2,1)} fusion(bf16[256,512]{1,0:T(8,128)(2,1)S(1)} %all_gather.7, bf16[1,512,1024]{2,1,0:T(8,128)(2,1)S(1)} %copy-done), kind=kOutput, calls=%fused_computation.3 | convolution fusion | flops 268697600 | bytes 1835008 | tf_op jit(solution)/shard_map/dot_general | solution.py:48
  66.1 5.5 %all-to-all-start.1 = ((bf16[8,32,1024]{2,1,0:T(8,128)(2,1)}), bf16[8,32,1024]{2,1,0:T(8,128)(2,1)S(1)}, u32[]{:S(2)}, u32[]{:S(2)}) async-start(bf16[8,32,1024]{2,1,0:T(8,128)(2,1)} %bitcast.8), calls=%async_computation.1 | async-start | bytes 1048576 | tf_op jit(solution)/shard_map/all_to_all | solution.py:54
  71.7 0.1 copy.12
  71.8 14.8 %all-to-all-done.1 = bf16[8,32,1024]{2,1,0:T(8,128)(2,1)S(1)} async-done(((bf16[8,32,1024]{2,1,0:T(8,128)(2,1)}), bf16[8,32,1024]{2,1,0:T(8,128)(2,1)S(1)}, u32[]{:S(2)}, u32[]{:S(2)}) %all-to-all-start.1) | async-done | bytes 524320 | tf_op jit(solution)/shard_map/all_to_all | solution.py:54
  86.6 1.2 %gather_fusion.1 = bf16[256,1024]{1,0:T(8,128)(2,1)S(1)} fusion(bf16[256,1024]{1,0:T(8,128)(2,1)S(1)} %bitcast.30, s32[1024]{0:T(1024)S(1)} %pad_clamp_fusion), kind=kCustom, calls=%fused_computation.1 | custom fusion | bytes 1049600 | tf_op jit(solution)/shard_map/gather | solution.py:56
  87.8 0.2 reshape.59
  88.0 0.7 fusion.10
  88.7 0.2 fusion.6
  88.9 5.9 %all-reduce.1 = (f32[128]{0:T(128)S(1)}, f32[128]{0:T(128)S(1)}) all-reduce(f32[128]{0:T(128)S(1)} %get-tuple-element.6, f32[128]{0:T(128)S(1)} %get-tuple-element.5), channel_id=1, replica_groups=mesh['ep'=8,'tp'=4] {'tp'}, use_global_device_ids=true, to_apply=%region_6.7 | all-reduce | flops 256 | bytes 2048 | tf_op jit(solution)/shard_map/psum | solution.py:62
  94.9 0.9 add_convert_fusion
  (29 shorter events, 0.2 us)
Async XLA Ops:
  6.5 58.3 %copy-start = (bf16[1,512,1024]{2,1,0:T(8,128)(2,1)S(1)}, bf16[1,512,1024]{2,1,0:T(8,128)(2,1)}, u32[]{:S(2)}) copy-start(bf16[1,512,1024]{2,1,0:T(8,128)(2,1)} %param.15) | copy-start | bytes 3145732
  6.5 49.3 %all-gather.2.cloned.1.call-start = ((), (), s32[]{:S(2)}) async-start(), calls=%async_computation.2 | async-start | bytes 2621440 | tf_op jit(solution)/shard_map/all_gather | solution.py:44
  11.1 44.7 %copy-start.3 = (bf16[1,4096,128]{2,1,0:T(8,128)(2,1)S(1)}, bf16[1,4096,128]{2,1,0:T(8,128)(2,1)}, u32[]{:S(2)}) copy-start(bf16[1,4096,128]{2,1,0:T(8,128)(2,1)} %param.13) | copy-start | bytes 3145732
  34.0 24.2 %copy-start.8 = (bf16[1,4096,128]{2,1,0:T(8,128)(2,1)S(1)}, bf16[1,4096,128]{2,1,0:T(8,128)(2,1)}, u32[]{:S(2)}) copy-start(bf16[1,4096,128]{2,1,0:T(8,128)(2,1)} %param.14) | copy-start | bytes 3145732
  55.8 2.5 %copy-start.2 = (bf16[256,4096]{1,0:T(8,128)(2,1)S(1)}, bf16[256,4096]{1,0:T(8,128)(2,1)}, u32[]{:S(2)}) copy-start(bf16[256,4096]{1,0:T(8,128)(2,1)} %all-gather.2.cloned.1.call-done) | copy-start | bytes 6291460
  59.0 12.6 %copy-start.6 = (f32[128,2]{0,1:T(2,128)S(1)}, f32[128,2]{0,1:T(2,128)}, u32[]{:S(2)}) copy-start(f32[128,2]{0,1:T(2,128)} %param.12) | copy-start | bytes 3076
  59.0 12.6 %copy-start.7 = (f32[128]{0:T(128)S(1)}, f32[128]{0:T(128)}, u32[]{:S(2)}) copy-start(f32[128]{0:T(128)} %param.11) | copy-start | bytes 1540
  66.1 20.5 %all-to-all-start.1 = ((bf16[8,32,1024]{2,1,0:T(8,128)(2,1)}), bf16[8,32,1024]{2,1,0:T(8,128)(2,1)S(1)}, u32[]{:S(2)}, u32[]{:S(2)}) async-start(bf16[8,32,1024]{2,1,0:T(8,128)(2,1)} %bitcast.8), calls=%async_computation.1 | async-start | bytes 1048576 | tf_op jit(solution)/shard_map/all_to_all | solution.py:54
  87.8 1.0 copy-start.1
  87.8 7.1 %copy-start.4 = (f32[1024]{0:T(1024)S(1)}, f32[1024]{0:T(1024)}, u32[]{:S(2)}) copy-start(f32[1024]{0:T(1024)} %param.17) | copy-start | bytes 12292
  87.8 7.1 %copy-start.5 = (f32[1024]{0:T(1024)S(1)}, f32[1024]{0:T(1024)}, u32[]{:S(2)}) copy-start(f32[1024]{0:T(1024)} %param.16) | copy-start | bytes 12292
Sparse Core Ops, SparseCore 0:
  34.2 21.5 all-gather.1
where the time goes:
time: 103 us
  waiting for transfers between devices  36.6 us (36%)
  blocking collectives  33.5 us (33%)
  between operations  13.6 us (13%)
  local copies, waits for them, and re-layouts  6.37 us (6%)
  starting transfers between devices  5.51 us (5%)
  matrix products  5.3 us (5%)
  other arithmetic  1.85 us (2%)
    all_gather x1, waiting for transfers between devices, on_device(): row_piece = lax.all_gather(row_block, 'tp', axis=1, tiled=True)  21.8 us
    all_to_all x1, blocking collectives, on_device(): lax.all_to_all(outgoing, 'ep', split_axis=0, concat_axis=0, tiled=True)  21.7 us
    all_to_all x1, waiting for transfers between devices, on_device(): lax.all_to_all(result, 'ep', split_axis=0, concat_axis=0, tiled=True)  14.8 us
    psum x1, blocking collectives, on_device(): lax.psum((jnp.sum(mixed, axis=1), jnp.sum(mixed * mixed, axis=1)), 'tp')  5.93 us
    all_gather x1, blocking collectives, on_device(): lax.all_gather(hidden, 'tp', axis=1, tiled=True)  5.81 us
    all_to_all x1, starting transfers between devices, on_device(): lax.all_to_all(result, 'ep', split_axis=0, concat_axis=0, tiled=True)  5.51 us
    dot_general x1, matrix products, on_device(): jnp.dot(row_piece, gate_local, preferred_element_type=jnp.float32)  2.45 us
  transfers between devices with their start and end apart: 2, of which 2 were waited for; matrix products, arithmetic and copies ran while one was open for 0% of the time, Pallas kernels for 0%

commit v1 on v0

--- a/solution.py
+++ b/solution.py
@@ -1,3 +1,4 @@
+import functools
 import jax
 import jax.numpy as jnp
 from jax import lax
@@ -8,6 +9,25 @@
 TOP_K = 2
 residual_scale = 2.0**0.5
 norm_eps = 1e-05
+
+
+def _take_pieces_all(w_in, row_dim):
+    n_all = lax.axis_size("tp")
+    latest = sorted(((src_i, (src_i + 1) % n_all) for src_i in range(n_all)))
+    row_out = w_in
+    all_rows = [row_out]
+    hop_no = 1
+    while hop_no < n_all:
+        row_out = lax.ppermute(row_out, "tp", latest)
+        all_rows.insert(0, row_out)
+        hop_no += 1
+    view_out = jnp.concatenate(all_rows, row_dim)
+    frame_out = lax.axis_index("tp")
+    w_next = frame_out + 1
+    return jnp.roll(view_out, w_next * w_in.shape[row_dim], row_dim)
+
+
+_solve_target = functools.partial(_take_pieces_all, row_dim=1)
 
 
 def on_device(
@@ -41,7 +61,7 @@
     arrived = lax.all_to_all(outgoing, "ep", split_axis=0, concat_axis=0, tiled=True)
     sources, slot_count, slice_width = arrived.shape
     row_block = arrived.reshape(sources * slot_count, slice_width)
-    row_piece = lax.all_gather(row_block, "tp", axis=1, tiled=True)
+    row_piece = _solve_target(row_block)
     gate_sum = jnp.dot(row_piece, gate_local, preferred_element_type=jnp.float32)
     up_sum = jnp.dot(row_piece, up_local, preferred_element_type=jnp.float32)
     hidden = (jax.nn.silu(gate_sum) * up_sum).astype(jnp.bfloat16)

time: 103 us -> 90.3 us (0.88)
  between operations: 13.6 us -> 0.22 us
  waiting for transfers between devices: 36.6 us -> 40.7 us
  starting transfers between devices: 5.51 us -> 3.6 us
  matrix products: 5.3 us -> 3.51 us
    ppermute x0 -> x3, waiting for transfers between devices: none -> 25.8 us  [_take_pieces_all(): row_out = lax.ppermute(row_out, 'tp', latest)]
    all_gather x1 -> x0, waiting for transfers between devices: 21.8 us -> none  [on_device(): row_piece = lax.all_gather(row_block, 'tp', axis=1, tiled=True)]
    all_to_all x1, starting transfers between devices: 5.51 us -> 3.6 us  [on_device(): lax.all_to_all(result, 'ep', split_axis=0, concat_axis=0, tiled=True)]
    dot_general x1, matrix products: 2.45 us -> 0.7 us  [on_device(): jnp.dot(row_piece, gate_local, preferred_element_type=jnp.float32)]
  transfers between devices with their start and end apart: 2 -> 4, of which waited for: 2 -> 4; matrix products, arithmetic and copies ran while one was open for 0% -> 0% of each run, Pallas kernels for 0% -> 0%
where the time goes in v1:
time: 90.3 us; the launch traced here: 90 us
  waiting for transfers between devices  40.7 us (45%)
  blocking collectives  33.2 us (37%)
  local copies, waits for them, and re-layouts  6.9 us (8%)
  starting transfers between devices  3.6 us (4%)
  matrix products  3.51 us (4%)
  other arithmetic  1.85 us (2%)
    ppermute x3, waiting for transfers between devices, _take_pieces_all(): row_out = lax.ppermute(row_out, 'tp', latest)  25.8 us
    all_to_all x1, blocking collectives, on_device(): lax.all_to_all(outgoing, 'ep', split_axis=0, concat_axis=0, tiled=True)  21.6 us
    all_to_all x1, waiting for transfers between devices, on_device(): lax.all_to_all(result, 'ep', split_axis=0, concat_axis=0, tiled=True)  14.9 us
    all_gather x1, blocking collectives, on_device(): lax.all_gather(hidden, 'tp', axis=1, tiled=True)  5.83 us
    psum x1, blocking collectives, on_device(): lax.psum((jnp.sum(mixed, axis=1), jnp.sum(mixed * mixed, axis=1)), 'tp')  5.77 us
    all_to_all x1, starting transfers between devices, on_device(): lax.all_to_all(result, 'ep', split_axis=0, concat_axis=0, tiled=True)  3.6 us
  transfers between devices with their start and end apart: 4, of which 4 were waited for; matrix products, arithmetic and copies ran while one was open for 0% of the time, Pallas kernels for 0%

profile of v1, /device:TPU:0, one launch (start us, length us, event | category | flops | bytes accessed | tf_op | source)
XLA Modules:
  0.0 90.0 jit_solution(2677183154476733930)
XLA Ops:
  0.0 0.9 copy.11
  0.9 0.7 broadcast_multiply_fusion
  1.7 0.2 fusion.4
  2.2 1.4 %scatter_custom_fusion = s32[256]{0:T(256)S(1)} fusion(s32[256]{0:T(256)S(1)} %bitcast.35, s32[256]{0:T(256)S(1)} %and_select_fusion, s32[]{:T(128)} %constant.54.clone.1), kind=kCustom, calls=%fused_computation.40 | custom fusion | bytes 1028 | tf_op jit(solution)/shard_map/scatter | solution.py:54
  3.6 1.0 %concatenate.9 = bf16[129,1024]{1,0:T(8,128)(2,1)S(1)} pad(bf16[128,1024]{1,0:T(8,128)(2,1)} %param.9, bf16[]{:T(256)} %constant.53.clone.1), padding=0_1x0_0 | pad | bytes 526338 | tf_op jit(solution)/shard_map/concatenate | solution.py:59
  4.6 1.2 %gather_fusion = bf16[256,1024]{1,0:T(8,128)(2,1)S(1)} fusion(bf16[129,1024]{1,0:T(8,128)(2,1)S(1)} %concatenate.9, s32[1024]{0:T(1024)S(1)} %pad_clamp_fusion.1), kind=kCustom, calls=%fused_computation | custom fusion | bytes 1049600 | tf_op jit(solution)/shard_map/gather | solution.py:60
  5.8 21.6 %all_to_all.10 = bf16[8,32,1024]{2,1,0:T(8,128)(2,1)S(1)} all-to-all(bf16[8,32,1024]{2,1,0:T(8,128)(2,1)S(1)} %bitcast.34), channel_id=1, replica_groups=mesh['ep'=8,'tp'=4] {'ep'}, dimensions={0} | all-to-all | bytes 1048576 | tf_op jit(solution)/shard_map/all_to_all | solution.py:61
  27.4 8.6 %collective-permute-done = bf16[256,1024]{1,0:T(8,128)(2,1)S(1)} collective-permute-done((bf16[256,1024]{1,0:T(8,128)(2,1)S(1)}, bf16[256,1024]{1,0:T(8,128)(2,1)S(1)}, u32[]{:S(2)}, u32[]{:S(2)}) %collective-permute-start) | collective-permute-done | bytes 524320 | tf_op jit(solution)/shard_map/ppermute | solution.py:21
  36.0 8.6 %collective-permute-done.1 = bf16[256,1024]{1,0:T(8,128)(2,1)S(1)} collective-permute-done((bf16[256,1024]{1,0:T(8,128)(2,1)S(1)}, bf16[256,1024]{1,0:T(8,128)(2,1)S(1)}, u32[]{:S(2)}, u32[]{:S(2)}) %collective-permute-start.1) | collective-permute-done | bytes 524320 | tf_op jit(solution)/shard_map/ppermute | solution.py:21
  44.6 8.6 %collective-permute-done.2 = bf16[256,1024]{1,0:T(8,128)(2,1)S(1)} collective-permute-done((bf16[256,1024]{1,0:T(8,128)(2,1)S(1)}, bf16[256,1024]{1,0:T(8,128)(2,1)S(1)}, u32[]{:S(2)}, u32[]{:S(2)}) %collective-permute-start.2) | collective-permute-done | bytes 524320 | tf_op jit(solution)/shard_map/ppermute | solution.py:21
  53.6 0.7 fusion.2
  54.3 0.3 copy-done.7
  54.6 0.7 multiply_convert_fusion
  55.3 5.8 %all_gather.3 = bf16[256,512]{1,0:T(8,128)(2,1)S(1)} all-gather(bf16[256,128]{1,0:T(8,128)(2,1)S(1)} %multiply_convert_fusion), channel_id=1, replica_groups=mesh['ep'=8,'tp'=4] {'tp'}, dimensions={1}, use_global_device_ids=true | all-gather | bytes 327680 | tf_op jit(solution)/shard_map/all_gather | solution.py:69
  61.1 1.2 %convolution_convert_fusion = bf16[256,1024]{1,0:T(8,128)(2,1)} fusion(bf16[256,512]{1,0:T(8,128)(2,1)S(1)} %all_gather.3, bf16[1,512,1024]{2,1,0:T(8,128)(2,1)S(1)} %copy-done), kind=kOutput, calls=%fused_computation.7 | convolution fusion | flops 268697600 | bytes 1835008 | tf_op jit(solution)/shard_map/dot_general | solution.py:68
  62.3 3.6 %all-to-all-start.1 = ((bf16[8,32,1024]{2,1,0:T(8,128)(2,1)}), bf16[8,32,1024]{2,1,0:T(8,128)(2,1)S(1)}, u32[]{:S(2)}, u32[]{:S(2)}) async-start(bf16[8,32,1024]{2,1,0:T(8,128)(2,1)} %bitcast.8), calls=%async_computation.1 | async-start | bytes 1048576 | tf_op jit(solution)/shard_map/all_to_all | solution.py:74
  66.0 0.1 copy.12
  66.1 14.9 %all-to-all-done.1 = bf16[8,32,1024]{2,1,0:T(8,128)(2,1)S(1)} async-done(((bf16[8,32,1024]{2,1,0:T(8,128)(2,1)}), bf16[8,32,1024]{2,1,0:T(8,128)(2,1)S(1)}, u32[]{:S(2)}, u32[]{:S(2)}) %all-to-all-start.1) | async-done | bytes 524320 | tf_op jit(solution)/shard_map/all_to_all | solution.py:74
  81.0 1.2 %gather_fusion.1 = bf16[256,1024]{1,0:T(8,128)(2,1)S(1)} fusion(bf16[256,1024]{1,0:T(8,128)(2,1)S(1)} %bitcast.30, s32[1024]{0:T(1024)S(1)} %pad_clamp_fusion), kind=kCustom, calls=%fused_computation.1 | custom fusion | bytes 1049600 | tf_op jit(solution)/shard_map/gather | solution.py:76
  82.2 0.2 reshape.59
  82.4 0.7 fusion.18
  83.1 0.2 fusion.8
  83.3 5.8 %all-reduce.1 = (f32[128]{0:T(128)S(1)}, f32[128]{0:T(128)S(1)}) all-reduce(f32[128]{0:T(128)S(1)} %get-tuple-element.6, f32[128]{0:T(128)S(1)} %get-tuple-element.5), channel_id=1, replica_groups=mesh['ep'=8,'tp'=4] {'tp'}, use_global_device_ids=true, to_apply=%region_6.7 | all-reduce | flops 256 | bytes 2048 | tf_op jit(solution)/shard_map/psum | solution.py:82
  89.1 0.9 %add_convert_fusion = bf16[128,1024]{1,0:T(8,128)(2,1)} fusion(f32[1024]{0:T(1024)S(1)} %copy-done.3, f32[1024]{0:T(1024)S(1)} %copy-done.4, f32[128]{0:T(128)S(1)} %get-tuple-element.10, f32[128]{0:T(128)S(1)} %get-tuple-element.9, f32[128,1,1024]{2,1,0:T(1,128)S(1)} %fusion.18, bf16[128,1024]{1,0:T(8,128)(2,1)S(1)} %copy-done.1), kind=kLoop, calls=%fused_computation.14 | loop fusion | flops 1048576 | bytes 1057792 | tf_op jit(solution)/shard_map/convert_element_type | solution.py:89
  (38 shorter events, 0.8 us)
Async XLA Ops:
  0.0 61.1 %copy-start = (bf16[1,512,1024]{2,1,0:T(8,128)(2,1)S(1)}, bf16[1,512,1024]{2,1,0:T(8,128)(2,1)}, u32[]{:S(2)}) copy-start(bf16[1,512,1024]{2,1,0:T(8,128)(2,1)} %param.15) | copy-start | bytes 3145732
  27.4 8.6 %collective-permute-start = (bf16[256,1024]{1,0:T(8,128)(2,1)S(1)}, bf16[256,1024]{1,0:T(8,128)(2,1)S(1)}, u32[]{:S(2)}, u32[]{:S(2)}) collective-permute-start(bf16[256,1024]{1,0:T(8,128)(2,1)S(1)} %bitcast.31), channel_id=1, source_target_pairs={{0,1},{1,2},{2,3},{3,0},{4,5},{5,6},{6,7},{7,4},{8,9},{9,10},{10,1... | collective-permute-start | bytes 1572872 | tf_op jit(solution)/shard_map/ppermute | solution.py:21
  36.0 8.6 %collective-permute-start.1 = (bf16[256,1024]{1,0:T(8,128)(2,1)S(1)}, bf16[256,1024]{1,0:T(8,128)(2,1)S(1)}, u32[]{:S(2)}, u32[]{:S(2)}) collective-permute-start(bf16[256,1024]{1,0:T(8,128)(2,1)S(1)} %collective-permute-done), channel_id=1, source_target_pairs={{0,1},{1,2},{2,3},{3,0},{4,5},{5,6},{6,7},{7,4},{8,9},{9,10},{10,1... | collective-permute-start | bytes 1572872 | tf_op jit(solution)/shard_map/ppermute | solution.py:21
  44.6 8.6 %collective-permute-start.2 = (bf16[256,1024]{1,0:T(8,128)(2,1)S(1)}, bf16[256,1024]{1,0:T(8,128)(2,1)S(1)}, u32[]{:S(2)}, u32[]{:S(2)}) collective-permute-start(bf16[256,1024]{1,0:T(8,128)(2,1)S(1)} %collective-permute-done.1), channel_id=1, source_target_pairs={{0,1},{1,2},{2,3},{3,0},{4,5},{5,6},{6,7},{7,4},{8,9},{9,10},{10,1... | collective-permute-start | bytes 1572872 | tf_op jit(solution)/shard_map/ppermute | solution.py:21
  44.6 9.0 %copy-start.2 = (bf16[1,4096,128]{2,1,0:T(8,128)(2,1)S(1)}, bf16[1,4096,128]{2,1,0:T(8,128)(2,1)}, u32[]{:S(2)}) copy-start(bf16[1,4096,128]{2,1,0:T(8,128)(2,1)} %param.13) | copy-start | bytes 3145732
  53.3 1.2 %copy-start.7 = (bf16[1,4096,128]{2,1,0:T(8,128)(2,1)S(1)}, bf16[1,4096,128]{2,1,0:T(8,128)(2,1)}, u32[]{:S(2)}) copy-start(bf16[1,4096,128]{2,1,0:T(8,128)(2,1)} %param.14) | copy-start | bytes 3145732
  54.5 11.4 %copy-start.5 = (f32[128,2]{0,1:T(2,128)S(1)}, f32[128,2]{0,1:T(2,128)}, u32[]{:S(2)}) copy-start(f32[128,2]{0,1:T(2,128)} %param.12) | copy-start | bytes 3076
  54.6 11.4 %copy-start.6 = (f32[128]{0:T(128)S(1)}, f32[128]{0:T(128)}, u32[]{:S(2)}) copy-start(f32[128]{0:T(128)} %param.11) | copy-start | bytes 1540
  62.3 18.7 %all-to-all-start.1 = ((bf16[8,32,1024]{2,1,0:T(8,128)(2,1)}), bf16[8,32,1024]{2,1,0:T(8,128)(2,1)S(1)}, u32[]{:S(2)}, u32[]{:S(2)}) async-start(bf16[8,32,1024]{2,1,0:T(8,128)(2,1)} %bitcast.8), calls=%async_computation.1 | async-start | bytes 1048576 | tf_op jit(solution)/shard_map/all_to_all | solution.py:74
  65.9 17.2 %copy-start.1 = (bf16[128,1024]{1,0:T(8,128)(2,1)S(1)}, bf16[128,1024]{1,0:T(8,128)(2,1)}, u32[]{:S(2)}) copy-start(bf16[128,1024]{1,0:T(8,128)(2,1)} %param.9) | copy-start | bytes 786436
  81.0 8.1 %copy-start.3 = (f32[1024]{0:T(1024)S(1)}, f32[1024]{0:T(1024)}, u32[]{:S(2)}) copy-start(f32[1024]{0:T(1024)} %param.17) | copy-start | bytes 12292
  81.0 8.1 %copy-start.4 = (f32[1024]{0:T(1024)S(1)}, f32[1024]{0:T(1024)}, u32[]{:S(2)}) copy-start(f32[1024]{0:T(1024)} %param.16) | copy-start | bytes 12292
